TPU v7x, 32 devices: a whole 2x2x4 slice. The times are simulated.
32 devices in a mesh: sp: 16 (over z, y, x), tp: 2 (over core).
Axes of the slice: x: 2, y: 2, z: 4, core: 2. Of those that a mesh axis runs over, the one named last changes fastest.
Arguments:
- receptance: bfloat16 [3072, 1024], P('sp', 'tp'), may hold values from -6 to 6
- head_keys: bfloat16 [3072, 1024], P('sp', 'tp'), may hold values from -6 to 6
- head_values: bfloat16 [3072, 1024], P('sp', 'tp'), may hold values from -6 to 6
- decay_preact: float32 [3072, 1024], P('sp', 'tp'), may hold values from -13.5 to -0.5
- learning_rate_preact: float32 [3072, 1024], P('sp', 'tp'), may hold values from -10.5 to 2.5
- output_gate_preact: bfloat16 [3072, 1024], P('sp', 'tp'), may hold values from -8 to 8
- self_token_weight: float32 [16, 64], P('tp'), may hold values from -0.6 to 0.6
- head_norm_gain: float32 [1024], P('tp'), may hold values from 0.1 to 1.9
- output_weight: bfloat16 [1024, 2048], P('tp'), may hold values from -0.1875 to 0.1875
- residual: bfloat16 [3072, 2048], P('sp'), may hold values from -6 to 6
- premixer_norm_gain: float32 [2048], replicated, may hold values from 0.1 to 1.9
- mixer_gate_weight: bfloat16 [2048, 5120], P('sp', 'tp'), may hold values from -0.125 to 0.125
- mixer_up_weight: bfloat16 [2048, 5120], P('sp', 'tp'), may hold values from -0.125 to 0.125
- mixer_down_weight: bfloat16 [5120, 2048], P('tp', 'sp'), may hold values from -0.078125 to 0.078125
Outputs:
- layer_out: bfloat16 [3072, 2048], P(('sp', 'tp'))
All inputs are finite; a program needn't handle non-finite values.
Results may differ from a plain program's by a relative error of at most 0.015.
Values may be sent and summed in bfloat16 or wider, within the bound.
A program may use at most 128 MiB of HBM per device.

v0:
```python
import jax
import jax.numpy as jnp
from jax import lax
from jax.sharding import PartitionSpec as P

HEAD_SIZE = 64
SUB = 16


GROUP_EPS = 0.00064
NORM_EPS = 1e-06
EXACT = lax.Precision.HIGHEST


def prefix(value, axis, join, neutral):
    count, mine = (lax.axis_size(axis), lax.axis_index(axis))
    pieces = jax.tree.map(lambda part: lax.all_gather(part, axis), value)
    running = jax.tree.map(
        lambda part, zero: jnp.full_like(part, 0) + jnp.asarray(zero, part.dtype), value, neutral
    )

    def turn(position, running):
        longer = join(running, jax.tree.map(lambda part: part[position], pieces))
        return jax.tree.map(lambda new, old: jnp.where(position < mine, new, old), longer, running)

    return lax.fori_loop(0, count - 1, turn, running)


def compose(earlier, latter):
    product = jnp.einsum("...ij,...jk->...ik", earlier[0], latter[0], precision=EXACT)
    carried = jnp.einsum("...ij,...jk->...ik", earlier[1], latter[0], precision=EXACT) + latter[1]
    return (product, carried)


def final_output(
    layer_result,
    receptance_rows,
    keys_single,
    values_single,
    self_token_weight,
    head_norm_gain,
    output_gate_preact,
):
    centre = jnp.mean(layer_result, axis=-1, keepdims=True)
    spread = jnp.mean(jnp.square(layer_result - centre), axis=-1, keepdims=True)
    scaled_rows = (layer_result - centre) * lax.rsqrt(spread + GROUP_EPS)
    self_token_term = (
        jnp.sum(receptance_rows * keys_single * self_token_weight[None], axis=-1, keepdims=True)
        * values_single
    )
    sequence_length = layer_result.shape[0]
    heads_merged = scaled_rows.reshape(sequence_length, -1) * head_norm_gain[
        None
    ] + self_token_term.reshape(sequence_length, -1)
    return (heads_merged * jax.nn.sigmoid(output_gate_preact.astype(jnp.float32))).astype(
        jnp.bfloat16
    )


def rms_scale(row_block, gain_vec):
    widened = row_block.astype(jnp.float32)
    factor = lax.rsqrt(jnp.mean(widened * widened, axis=-1, keepdims=True) + NORM_EPS)
    return (widened * factor * gain_vec[None]).astype(jnp.bfloat16)


def per_device(
    receptance,
    head_keys,
    head_values,
    decay_preact,
    learning_rate_preact,
    output_gate_preact,
    self_token_weight,
    head_norm_gain,
    output_weight,
    residual,
    premixer_norm_gain,
    mixer_gate_weight,
    mixer_up_weight,
    mixer_down_weight,
):
    sequence_length = receptance.shape[0]
    head_count = receptance.shape[1] // HEAD_SIZE
    blocks = sequence_length // SUB
    layout = (sequence_length, head_count, HEAD_SIZE)
    receptance_rows = receptance.astype(jnp.float32).reshape(layout)
    keys_single = head_keys.astype(jnp.float32).reshape(layout)
    values_single = head_values.astype(jnp.float32).reshape(layout)
    decay_rate = jnp.exp(-jnp.exp(-jax.nn.softplus(-decay_preact) - 0.5)).reshape(layout)
    learn_rate = jax.nn.sigmoid(learning_rate_preact).reshape(layout)
    unit_key = keys_single / jnp.maximum(jnp.linalg.norm(keys_single, axis=-1, keepdims=True), 1.0)
    remove_dir = -unit_key
    insert_dir = unit_key * learn_rate

    def split_time(values_in):
        return jnp.swapaxes(values_in.reshape(blocks, SUB, head_count, HEAD_SIZE), 0, 1)

    series = tuple(
        (
            split_time(member)
            for member in (
                decay_rate,
                keys_single,
                values_single,
                remove_dir,
                insert_dir,
                receptance_rows,
            )
        )
    )
    head_eye = jnp.broadcast_to(
        jnp.eye(HEAD_SIZE, dtype=jnp.float32), (head_count, HEAD_SIZE, HEAD_SIZE)
    )
    block_eye = jnp.broadcast_to(head_eye[None], (blocks, head_count, HEAD_SIZE, HEAD_SIZE))

    def advance(current, inputs):
        product, memory = current
        decay_t, key_t, value_t, remove_t, insert_t, recept_t = inputs
        shifted = jnp.einsum("bhij,bhj->bhi", product, remove_t, precision=EXACT)
        product = product * decay_t[:, :, None, :] + shifted[..., None] * insert_t[:, :, None, :]
        erased = jnp.einsum("bhij,bhj->bhi", memory, remove_t, precision=EXACT)
        memory = (
            memory * decay_t[:, :, None, :]
            + erased[..., None] * insert_t[:, :, None, :]
            + value_t[..., None] * key_t[:, :, None, :]
        )
        seen_part = jnp.einsum("bhij,bhj->bhi", product, recept_t, precision=EXACT)
        local_part = jnp.einsum("bhij,bhj->bhi", memory, recept_t, precision=EXACT)
        return ((product, memory), (seen_part, local_part))

    (block_prod, block_state), (seen_part, local_part) = lax.scan(
        advance, (block_eye, jnp.zeros_like(block_eye)), series
    )
    inclusive = lax.associative_scan(compose, (block_prod, block_state), axis=0)
    before_prod = jnp.concatenate([head_eye[None], inclusive[0][:-1]], axis=0)
    before_state = jnp.concatenate([jnp.zeros_like(head_eye)[None], inclusive[1][:-1]], axis=0)
    totals = (inclusive[0][-1], inclusive[1][-1])
    incoming = prefix(totals, "sp", compose, (head_eye, jnp.zeros_like(head_eye)))[1]
    entry_state = (
        jnp.einsum("hij,bhjk->bhik", incoming, before_prod, precision=EXACT) + before_state
    )
    joined = jnp.einsum("bhij,tbhj->tbhi", entry_state, seen_part, precision=EXACT) + local_part
    recurrence_output = jnp.swapaxes(joined, 0, 1).reshape(layout)
    mixer_output = final_output(
        recurrence_output,
        receptance_rows,
        keys_single,
        values_single,
        self_token_weight,
        head_norm_gain,
        output_gate_preact,
    )
    own_rows = sequence_length // lax.axis_size("tp")
    row_start = lax.axis_index("tp") * own_rows
    mix_sum = lax.psum_scatter(
        jnp.dot(mixer_output, output_weight, preferred_element_type=jnp.float32).astype(
            jnp.bfloat16
        ),
        "tp",
        scatter_dimension=0,
        tiled=True,
    )
    mix = lax.optimization_barrier(mix_sum).astype(jnp.float32)
    resid_rows = lax.dynamic_slice_in_dim(residual, row_start, own_rows, 0)
    after_mix = (resid_rows.astype(jnp.float32) + mix).astype(jnp.bfloat16)
    normed = lax.all_gather(rms_scale(after_mix, premixer_norm_gain), "tp", axis=0, tiled=True)
    gate_more = jnp.dot(
        normed,
        lax.all_gather(mixer_gate_weight, "sp", axis=0, tiled=True),
        preferred_element_type=jnp.float32,
    )
    up_more = jnp.dot(
        normed,
        lax.all_gather(mixer_up_weight, "sp", axis=0, tiled=True),
        preferred_element_type=jnp.float32,
    )
    hidden = (jax.nn.silu(gate_more) * up_more).astype(jnp.bfloat16)
    down_full = lax.all_gather(mixer_down_weight, "sp", axis=1, tiled=True)
    down_sum = lax.psum_scatter(
        jnp.dot(hidden, down_full, preferred_element_type=jnp.float32).astype(jnp.bfloat16),
        "tp",
        scatter_dimension=0,
        tiled=True,
    ).astype(jnp.float32)
    return (after_mix.astype(jnp.float32) + down_sum).astype(jnp.bfloat16)


def solution(mesh):
    placed = (
        P("sp", "tp"),
        P("sp", "tp"),
        P("sp", "tp"),
        P("sp", "tp"),
        P("sp", "tp"),
        P("sp", "tp"),
        P("tp", None),
        P("tp"),
        P("tp", None),
        P("sp", None),
        P(),
        P("sp", "tp"),
        P("sp", "tp"),
        P("tp", "sp"),
    )
    return jax.shard_map(
        per_device, mesh=mesh, in_specs=placed, out_specs=P(("sp", "tp"), None), check_vma=False
    )
```

profile of v0, /device:TPU:15, one launch (start us, length us, event | category | flops | bytes accessed | tf_op | source)
XLA Modules:
  0.0 1479.3 jit_solution(12337967907112899580)
XLA Ops:
  24.4 669.8 %while.31 = (s32[]{:T(128)}, f32[12,8,64,64]{3,2,1,0:T(8,128)}, f32[12,8,64,64]{3,2,1,0:T(8,128)}, f32[16,12,8,64]{3,0,2,1:T(8,128)}, f32[16,12,8,64]{3,0,2,1:T(...) while((s32[]{:T(128)}, f32[12,8,64,64]{3,2,1,0:T(8,128)}, ...), condition=%wide.region_2.3_spmd.clone, body=%wide.region_1.2_spmd.clone.sunk | while | flops 22806532 | bytes 25903316 | solution.py:131
  65.3 7.0 fusion.115
  107.3 7.0 fusion.115
  149.2 7.0 fusion.115
  191.2 7.0 fusion.115
  401.0 7.0 fusion.115
  714.2 8.6 pad.48
  725.7 8.5 pad.47
  740.4 24.4 %pad.50 = f32[12,8,64,64]{3,2,1,0:T(8,128)} pad(f32[6,8,64,64]{3,2,1,0:T(8,128)} %copy-done.5, f32[]{:T(128)} %constant.72.clone.1), padding=1_0_1x0_0_0x0_0_0x0_0_0 | pad | bytes 2359300 | tf_op jit(solution)/shard_map/pad | solution.py:134
  767.1 24.5 %pad.49 = f32[12,8,64,64]{3,2,1,0:T(8,128)} pad(f32[6,8,64,64]{3,2,1,0:T(8,128)} %pad_maximum_fusion.1, f32[]{:T(128)} %constant.72.clone.1), padding=0_1_1x0_0_0x0_0_0x0_0_0 | pad | bytes 2359300 | tf_op jit(solution)/shard_map/pad | solution.py:134
  801.3 8.5 pad.42
  811.6 8.6 pad.41
  823.9 24.4 %pad.92 = f32[11,8,64,64]{3,2,1,0:T(8,128)} pad(f32[6,8,64,64]{3,2,1,0:T(8,128)} %add.167, f32[]{:T(128)} %constant.72.clone.1), padding=0_0_1x0_0_0x0_0_0x0_0_0 | pad | bytes 2228228
  850.0 24.4 %pad.67 = f32[11,8,64,64]{3,2,1,0:T(8,128)} pad(f32[6,8,64,64]{3,2,1,0:T(8,128)} %pad_maximum_fusion.1, f32[]{:T(128)} %constant.72.clone.1), padding=0_0_1x0_0_0x0_0_0x0_0_0 | pad | bytes 2228228 | tf_op jit(solution)/shard_map/slice | solution.py:136
  875.4 24.5 %pad.44 = f32[12,8,64,64]{3,2,1,0:T(8,128)} pad(f32[6,8,64,64]{3,2,1,0:T(8,128)} %add.167, f32[]{:T(128)} %constant.72.clone.1), padding=1_0_1x0_0_0x0_0_0x0_0_0 | pad | bytes 2359300 | tf_op jit(solution)/shard_map/pad | solution.py:134
  904.4 24.4 %pad.43 = f32[12,8,64,64]{3,2,1,0:T(8,128)} pad(f32[6,8,64,64]{3,2,1,0:T(8,128)} %pad_maximum_fusion, f32[]{:T(128)} %constant.72.clone.1), padding=0_1_1x0_0_0x0_0_0x0_0_0 | pad | bytes 2359300 | tf_op jit(solution)/shard_map/pad | solution.py:134
  945.1 40.9 %while.32 = (s32[]{:T(128)}, f32[8,64,64]{1,2,0:T(8,128)S(1)}, s32[]{:T(128)}, f32[16,8,64,64]{3,2,1,0:T(8,128)}, f32[16,8,64,64]{3,2,1,0:T(8,128)}, /*index=5*/s32[]{:T(128)}, s32[]{:T(128)}) while((s32[]{:T(128)}, f32[8,64,64]{1,2,0:T(8,128)S(1)}, s32[]{:T(128)}, f32[16,8,64,64]{3,2,1,0:T(8,128)}, f32[16,8,64,64]{3,2,1,0:T(8,128)}, ...), condition=%wide.region_4.5_spmd.clone, body=%wide.region_3.4_spmd.clone.sunk | while | flops 25296900 | bytes 1968227 | solution.py:26
  1006.3 7.9 reduce-scatter.3.cloned.1.call-done
  1018.4 126.8 %all-gather.10.cloned.1.call-done = bf16[2048,2560]{1,0:T(8,128)(2,1)} async-done(((bf16[128,2560]{1,0:T(8,128)(2,1)}), bf16[2048,2560]{1,0:T(8,128)(2,1)}) %all-gather.10.cloned.1.call-update) | async-done | bytes 10485776 | tf_op jit(solution)/shard_map/all_gather | solution.py:169
  1145.2 7.5 fusion.74
  1152.6 124.8 %all-gather.12.cloned.1.call-done = bf16[2048,2560]{1,0:T(8,128)(2,1)} async-done(((bf16[128,2560]{1,0:T(8,128)(2,1)}), bf16[2048,2560]{1,0:T(8,128)(2,1)}) %all-gather.12.cloned.1.call-update) | async-done | bytes 10485776 | tf_op jit(solution)/shard_map/all_gather | solution.py:174
  1277.4 169.4 %all-gather.14.cloned.1.call-done = bf16[2560,2048]{1,0:T(8,128)(2,1)} async-done(((bf16[2560,128]{1,0:T(8,128)(2,1)}), bf16[2560,2048]{1,0:T(8,128)(2,1)}) %all-gather.14.cloned.1.call-update) | async-done | bytes 10485776 | tf_op jit(solution)/shard_map/all_gather | solution.py:178
  1446.9 12.8 convolution_convert_fusion
  1459.7 10.7 reduce-scatter.5.cloned.1.call-done
  (416 shorter events, 787.7 us)
Async XLA Ops:
  6.5 995.2 %copy-start = (bf16[512,2048]{1,0:T(8,128)(2,1)S(1)}, bf16[512,2048]{1,0:T(8,128)(2,1)}, u32[]{:S(2)}) copy-start(bf16[512,2048]{1,0:T(8,128)(2,1)} %param.26) | copy-start | bytes 6291460
  6.5 931.7 %all-gather.8.cloned.1.call-start = ((), (), s32[]{:S(2)}) async-start(), calls=%async_computation.3 | async-start | bytes 4456448 | tf_op jit(solution)/shard_map/all_gather | solution.py:17
  65.3 15.6 %copy-start.1 = (f32[12,8,64,64]{3,2,1,0:T(8,128)S(1)}, f32[12,8,64,64]{3,2,1,0:T(8,128)}, u32[]{:S(2)}) copy-start(f32[12,8,64,64]{3,2,1,0:T(8,128)} %get-tuple-element.448) | copy-start | bytes 4718596 | tf_op jit(solution)/shard_map/while
  107.3 15.6 %copy-start.1 = (f32[12,8,64,64]{3,2,1,0:T(8,128)S(1)}, f32[12,8,64,64]{3,2,1,0:T(8,128)}, u32[]{:S(2)}) copy-start(f32[12,8,64,64]{3,2,1,0:T(8,128)} %get-tuple-element.448) | copy-start | bytes 4718596 | tf_op jit(solution)/shard_map/while
  149.2 15.6 %copy-start.1 = (f32[12,8,64,64]{3,2,1,0:T(8,128)S(1)}, f32[12,8,64,64]{3,2,1,0:T(8,128)}, u32[]{:S(2)}) copy-start(f32[12,8,64,64]{3,2,1,0:T(8,128)} %get-tuple-element.448) | copy-start | bytes 4718596 | tf_op jit(solution)/shard_map/while
  191.2 15.6 %copy-start.1 = (f32[12,8,64,64]{3,2,1,0:T(8,128)S(1)}, f32[12,8,64,64]{3,2,1,0:T(8,128)}, u32[]{:S(2)}) copy-start(f32[12,8,64,64]{3,2,1,0:T(8,128)} %get-tuple-element.448) | copy-start | bytes 4718596 | tf_op jit(solution)/shard_map/while
  233.2 15.6 %copy-start.1 = (f32[12,8,64,64]{3,2,1,0:T(8,128)S(1)}, f32[12,8,64,64]{3,2,1,0:T(8,128)}, u32[]{:S(2)}) copy-start(f32[12,8,64,64]{3,2,1,0:T(8,128)} %get-tuple-element.448) | copy-start | bytes 4718596 | tf_op jit(solution)/shard_map/while
  275.1 15.6 %copy-start.1 = (f32[12,8,64,64]{3,2,1,0:T(8,128)S(1)}, f32[12,8,64,64]{3,2,1,0:T(8,128)}, u32[]{:S(2)}) copy-start(f32[12,8,64,64]{3,2,1,0:T(8,128)} %get-tuple-element.448) | copy-start | bytes 4718596 | tf_op jit(solution)/shard_map/while
  317.1 15.6 %copy-start.1 = (f32[12,8,64,64]{3,2,1,0:T(8,128)S(1)}, f32[12,8,64,64]{3,2,1,0:T(8,128)}, u32[]{:S(2)}) copy-start(f32[12,8,64,64]{3,2,1,0:T(8,128)} %get-tuple-element.448) | copy-start | bytes 4718596 | tf_op jit(solution)/shard_map/while
  401.0 15.6 %copy-start.1 = (f32[12,8,64,64]{3,2,1,0:T(8,128)S(1)}, f32[12,8,64,64]{3,2,1,0:T(8,128)}, u32[]{:S(2)}) copy-start(f32[12,8,64,64]{3,2,1,0:T(8,128)} %get-tuple-element.448) | copy-start | bytes 4718596 | tf_op jit(solution)/shard_map/while
  442.9 15.6 %copy-start.1 = (f32[12,8,64,64]{3,2,1,0:T(8,128)S(1)}, f32[12,8,64,64]{3,2,1,0:T(8,128)}, u32[]{:S(2)}) copy-start(f32[12,8,64,64]{3,2,1,0:T(8,128)} %get-tuple-element.448) | copy-start | bytes 4718596 | tf_op jit(solution)/shard_map/while
  484.9 15.6 %copy-start.1 = (f32[12,8,64,64]{3,2,1,0:T(8,128)S(1)}, f32[12,8,64,64]{3,2,1,0:T(8,128)}, u32[]{:S(2)}) copy-start(f32[12,8,64,64]{3,2,1,0:T(8,128)} %get-tuple-element.448) | copy-start | bytes 4718596 | tf_op jit(solution)/shard_map/while
  568.8 15.6 %copy-start.1 = (f32[12,8,64,64]{3,2,1,0:T(8,128)S(1)}, f32[12,8,64,64]{3,2,1,0:T(8,128)}, u32[]{:S(2)}) copy-start(f32[12,8,64,64]{3,2,1,0:T(8,128)} %get-tuple-element.448) | copy-start | bytes 4718596 | tf_op jit(solution)/shard_map/while
  610.8 15.6 %copy-start.1 = (f32[12,8,64,64]{3,2,1,0:T(8,128)S(1)}, f32[12,8,64,64]{3,2,1,0:T(8,128)}, u32[]{:S(2)}) copy-start(f32[12,8,64,64]{3,2,1,0:T(8,128)} %get-tuple-element.448) | copy-start | bytes 4718596 | tf_op jit(solution)/shard_map/while
  767.1 26.3 %copy-start.11 = (f32[3,8,64,64]{3,2,1,0:T(8,128)S(1)}, f32[3,8,64,64]{3,2,1,0:T(8,128)}, u32[]{:S(2)}) copy-start(f32[3,8,64,64]{3,2,1,0:T(8,128)} %copy-done.10) | copy-start | bytes 1179652
  767.1 27.1 %slice-start.1 = ((f32[3,8,64,64]{3,2,1,0:T(8,128)}), f32[1,8,64,64]{3,2,1,0:T(8,128)S(1)}, s32[]{:S(2)}) async-start(f32[3,8,64,64]{3,2,1,0:T(8,128)} %copy-done.10), calls=%async_computation.10 | async-start | bytes 524288 | tf_op jit(solution)/shard_map/slice | solution.py:134
  793.3 151.7 %all-gather.6.cloned.1.call-start = ((), (), s32[]{:S(2)}) async-start(), calls=%async_computation.2 | async-start | bytes 4456448 | tf_op jit(solution)/shard_map/all_gather | solution.py:17
  850.0 164.3 %reduce-scatter.3.cloned.1.call-start = ((), (), s32[]{:S(2)}) async-start(), calls=%async_computation.4 | async-start | bytes 1179648 | tf_op jit(solution)/shard_map/reduce_scatter | solution.py:155
  904.4 24.4 %copy-start.14 = (f32[192,512]{1,0:T(8,128)S(1)}, f32[192,512]{1,0:T(8,128)}, u32[]{:S(2)}) copy-start(f32[192,512]{1,0:T(8,128)} %get-tuple-element.316) | copy-start | bytes 1179652
  904.4 24.6 %copy-start.20 = (f32[8,64]{1,0:T(8,128)S(1)}, f32[8,64]{1,0:T(8,128)}, u32[]{:S(2)}) copy-start(f32[8,64]{1,0:T(8,128)} %param.24) | copy-start | bytes 6148
  1004.5 140.7 %all-gather.10.cloned.1.call-start = ((), (), s32[]{:S(2)}) async-start(), calls=%async_computation.5 | async-start | bytes 11141120 | tf_op jit(solution)/shard_map/all_gather | solution.py:169
  1005.1 272.3 %all-gather.12.cloned.1.call-start = ((), (), s32[]{:S(2)}) async-start(), calls=%async_computation.6 | async-start | bytes 11141120 | tf_op jit(solution)/shard_map/all_gather | solution.py:174
  1005.7 441.2 %all-gather.14.cloned.1.call-start = ((), (), s32[]{:S(2)}) async-start(), calls=%async_computation.7 | async-start | bytes 11141120 | tf_op jit(solution)/shard_map/all_gather | solution.py:178
  1006.3 464.1 %reduce-scatter.5.cloned.1.call-start = ((), (), s32[]{:S(2)}) async-start(), calls=%async_computation.8 | async-start | bytes 1179648 | tf_op jit(solution)/shard_map/reduce_scatter | solution.py:179
  (38 other events, 184.6 us)
Sparse Core Ops, SparseCore 0:
  793.5 74.5 all-gather.7
  870.8 74.1 all-gather.5
  1004.6 9.5 reduce-scatter.2
  1016.8 128.3 all-gather.9
  1147.7 129.6 all-gather.11
  1280.0 166.8 all-gather.13
  1459.8 10.5 reduce-scatter.4
where the time goes:
time: 1510 us; the launch traced here: 1480 us
  matrix products  487 us (32%)
  waiting for transfers between devices  448 us (30%)
  local copies, waits for them, and re-layouts  384 us (25%)
  other arithmetic  141 us (9%)
    all_gather x1, waiting for transfers between devices, per_device(): down_full = lax.all_gather(mixer_down_weight, 'sp', axis=1, tiled=True)  169 us
    pad x10, local copies, waits for them, and re-layouts, per_device(): inclusive = lax.associative_scan(compose, (block_prod, block_state), axis=0)  144 us
    all_gather x1, waiting for transfers between devices, per_device(): lax.all_gather(mixer_gate_weight, 'sp', axis=0, tiled=True)  127 us
    all_gather x1, waiting for transfers between devices, per_device(): lax.all_gather(mixer_up_weight, 'sp', axis=0, tiled=True)  125 us
    dot_general x16, matrix products, advance(): erased = jnp.einsum('bhij,bhj->bhi', memory, remove_t, precision=EXACT)  110 us
    dot_general x16, matrix products, advance(): shifted = jnp.einsum('bhij,bhj->bhi', product, remove_t, precision=EXACT)  110 us
    dot_general x16, matrix products, advance(): seen_part = jnp.einsum('bhij,bhj->bhi', product, recept_t, precision=EXACT)  110 us
    add x16, other arithmetic, advance(): memory * decay_t[:, :, None, :]  106 us
  transfers between devices with their start and end apart: 7, of which 6 were waited for; matrix products, arithmetic and copies ran while one was open for 10% of the time, Pallas kernels for 0%

commit v1 on v0

v1 whole, which is shorter than its diff:
```python
import functools

import jax
import jax.numpy as jnp
from jax import lax
from jax.experimental import pallas as pl
from jax.experimental.pallas import tpu as pltpu
from jax.sharding import PartitionSpec as P

HEAD = 64
LANES = 2 * HEAD
GROUP_EPS = 0.00064
NORM_EPS = 1e-06
NN = (((1,), (0,)), ((), ()))
NT = (((1,), (1,)), ((), ()))
TN = (((0,), (0,)), ((), ()))
INNER = 4


def split(x):
    high = x.astype(jnp.bfloat16)
    return high, (x - high.astype(jnp.float32)).astype(jnp.bfloat16)


def dot1(a, b, dims=NN):
    return lax.dot_general(
        a.astype(jnp.bfloat16), b.astype(jnp.bfloat16), dims, preferred_element_type=jnp.float32
    )


def dot3(a, b, dims=NN):
    ah, al = a if isinstance(a, tuple) else split(a)
    bh, bl = b if isinstance(b, tuple) else split(b)
    d = functools.partial(
        lax.dot_general, dimension_numbers=dims, preferred_element_type=jnp.float32
    )
    return d(ah, bh) + (d(ah, bl) + d(al, bh))


def per_head_sum(x, first):
    s0 = jnp.sum(jnp.where(first, x, 0.0), axis=-1, keepdims=True)
    s1 = jnp.sum(jnp.where(first, 0.0, x), axis=-1, keepdims=True)
    return jnp.where(first, s0, s1)


def block_diag_mask():
    row = lax.broadcasted_iota(jnp.int32, (LANES, LANES), 0)
    col = lax.broadcasted_iota(jnp.int32, (LANES, LANES), 1)
    return row // HEAD == col // HEAD, row == col


def fold(full):
    mask, _ = block_diag_mask()
    kept = jnp.where(mask, full, 0.0)
    return kept[:HEAD] + kept[HEAD:]


def unfold(packed):
    mask, _ = block_diag_mask()
    return jnp.where(mask, jnp.concatenate([packed, packed], axis=0), 0.0)


def local_kernel(r_ref, k_ref, v_ref, dw_ref, lw_ref, q_ref, y_ref, ps_ref):
    steps = r_ref.shape[0]
    f32 = jnp.float32
    first = lax.broadcasted_iota(jnp.int32, (steps, LANES), 1) < HEAD
    row = lax.broadcasted_iota(jnp.int32, (steps, steps), 0)
    col = lax.broadcasted_iota(jnp.int32, (steps, steps), 1)
    r, k, v = (x[...].astype(f32) for x in (r_ref, k_ref, v_ref))
    log_decay = jax.nn.sigmoid(dw_ref[...]) * (-0.6065306597126334)
    ones = (row >= col).astype(jnp.bfloat16)
    h0 = log_decay.astype(jnp.bfloat16)
    rest = log_decay - h0.astype(f32)
    h1 = rest.astype(jnp.bfloat16)
    h2 = (rest - h1.astype(f32)).astype(jnp.bfloat16)
    total = dot1(ones, h0) + (dot1(ones, h1) + dot1(ones, h2))
    last = total[steps - 1 :, :]
    unit = k / jnp.maximum(jnp.sqrt(per_head_sum(k * k, first)), 1.0)
    insert = unit * jax.nn.sigmoid(lw_ref[...])
    undo = jnp.exp(-total)
    remaining = jnp.exp(last - total)
    a_bar = -unit * jnp.exp(total - log_decay)
    r_bar = r * jnp.exp(total)
    b_hat = insert * undo
    k_hat = k * undo
    right = split(jnp.concatenate([b_hat, k_hat], axis=0))
    left = jnp.concatenate([a_bar, r_bar], axis=0)
    first2 = jnp.concatenate([first, first], axis=0)
    grams = [
        dot3(jnp.where(first2 if h == 0 else ~first2, left, 0.0), right, NT) for h in (0, 1)
    ]
    strict, incl = row > col, row >= col
    ab = [jnp.where(strict, g[:steps, :steps], 0.0) for g in grams]
    ak = [jnp.where(strict, g[:steps, steps:], 0.0) for g in grams]
    rb = [jnp.where(incl, g[steps:, :steps], 0.0) for g in grams]
    rk = [jnp.where(incl, g[steps:, steps:], 0.0) for g in grams]
    vb = v_ref[...]

    def times_v(m):
        mh, ml = split(m)
        return dot1(mh, vb) + dot1(ml, vb)

    seeds = [jnp.concatenate([a_bar, times_v(m)], axis=1) for m in ak]
    ab16 = [m.astype(jnp.bfloat16) for m in ab]
    eye = (row == col).astype(f32)
    size = 1
    inv = None
    while size < steps:
        joined = (
            (row // (2 * size) == col // (2 * size))
            & ((row // size) % 2 == 1)
            & ((col // size) % 2 == 0)
        )
        parts = [jnp.where(joined, m, jnp.zeros_like(m)) for m in ab16]
        if inv is None:
            inv = [eye + p.astype(f32) for p in parts]
        else:
            t16 = [t.astype(jnp.bfloat16) for t in inv]
            mid = [dot1(t, p) for t, p in zip(t16, parts)]
            inv = [t + dot1(m, tt) for t, m, tt in zip(inv, mid, t16)]
        size *= 2
    inv16 = [t.astype(jnp.bfloat16) for t in inv]
    absp = [split(m) for m in ab]
    sol = [dot1(t, s) for t, s in zip(inv16, seeds)]
    for _ in range(2):
        res = [s - x + dot3(m, x) for s, x, m in zip(seeds, sol, absp)]
        sol = [x + dot1(t, e) for x, t, e in zip(sol, inv16, res)]
    outs = [dot3(m, x) for m, x in zip(rb, sol)]
    own = [times_v(m) for m in rk]
    q_ref[...] = r_bar + jnp.where(first, outs[0][:, :LANES], outs[1][:, :LANES])
    y_ref[...] = jnp.where(first, outs[0][:, LANES:] + own[0], outs[1][:, LANES:] + own[1])
    w = jnp.where(first, sol[0][:, :LANES], sol[1][:, :LANES])
    u = jnp.where(first, sol[0][:, LANES:], sol[1][:, LANES:])
    b_end = split(insert * remaining)
    _, diag = block_diag_mask()
    prod = dot3(w, b_end, TN) + jnp.where(diag, jnp.exp(last), 0.0)
    kh, kl = split(k * remaining)
    state = dot3(u, b_end, TN) + dot1(vb, kh, TN) + dot1(vb, kl, TN)
    ps_ref[0, 0] = fold(prod)
    ps_ref[0, 1] = fold(state)


def join_kernel(i_ref, ps_ref, q_ref, y_ref, r_ref, k_ref, v_ref, g_ref, tw_ref, hg_ref, w_ref, o_ref):
    steps = q_ref.shape[0]
    pairs = q_ref.shape[1] // LANES
    f32 = jnp.float32
    first = lax.broadcasted_iota(jnp.int32, (steps, LANES), 1) < HEAD

    def turn(j, states):
        return tuple(
            dot3(s, unfold(ps_ref[j, p, 0])) + unfold(ps_ref[j, p, 1])
            for p, s in enumerate(states)
        )

    zero = jnp.zeros((LANES, LANES), f32)
    states = lax.fori_loop(0, i_ref[0], turn, (zero,) * pairs)
    mixed = []
    for p in range(pairs):
        cut = slice(p * LANES, (p + 1) * LANES)
        y = dot3(q_ref[:, cut], states[p], NT) + y_ref[:, cut]
        y = y - per_head_sum(y, first) * (1.0 / HEAD)
        spread = per_head_sum(y * y, first) * (1.0 / HEAD)
        r, k, v = (x[:, cut].astype(f32) for x in (r_ref, k_ref, v_ref))
        own = per_head_sum(r * k * tw_ref[:, cut], first) * v
        out = y * lax.rsqrt(spread + GROUP_EPS) * hg_ref[:, cut] + own
        mixed.append((out * jax.nn.sigmoid(g_ref[:, cut].astype(f32))).astype(jnp.bfloat16))
    mixed = jnp.concatenate(mixed, axis=1)
    o_ref[...] = jnp.dot(mixed, w_ref[...], preferred_element_type=f32).astype(jnp.bfloat16)


def recurrence(r, k, v, dw, lw):
    steps, width = r.shape
    pairs = width // LANES
    cols = pl.BlockSpec((steps, LANES), lambda p: (0, p))
    return pl.pallas_call(
        local_kernel,
        grid=(pairs,),
        in_specs=[cols] * 5,
        out_specs=[cols, cols, pl.BlockSpec((1, 2, HEAD, LANES), lambda p: (p, 0, 0, 0))],
        out_shape=[
            jax.ShapeDtypeStruct((steps, width), jnp.float32),
            jax.ShapeDtypeStruct((steps, width), jnp.float32),
            jax.ShapeDtypeStruct((pairs, 2, HEAD, LANES), jnp.float32),
        ],
        cost_estimate=pl.CostEstimate(
            flops=20_000_000_000, bytes_accessed=4_000_000, transcendentals=1_000_000
        ),
        name="local_part",
    )(r, k, v, dw, lw)


def join(index, ps, q, y, r, k, v, gate, tw, hg, w):
    vmem = pl.BlockSpec(memory_space=pltpu.VMEM)
    return pl.pallas_call(
        join_kernel,
        in_specs=[pl.BlockSpec(memory_space=pltpu.SMEM)] + [vmem] * 10,
        out_specs=vmem,
        out_shape=jax.ShapeDtypeStruct((q.shape[0], w.shape[1]), jnp.bfloat16),
        cost_estimate=pl.CostEstimate(
            flops=10_000_000_000, bytes_accessed=8_000_000, transcendentals=100_000
        ),
        name="join_part",
    )(index, ps, q, y, r, k, v, gate, tw, hg, w)


def rms_scale(rows, gain):
    x = rows.astype(jnp.float32)
    factor = lax.rsqrt(jnp.mean(x * x, axis=-1, keepdims=True) + NORM_EPS)
    return (x * factor * gain[None]).astype(jnp.bfloat16)


def per_device(r, k, v, dw, lw, gate, tw, hg, w_out, residual, gain, w_gate, w_up, w_down):
    steps = r.shape[0]
    sp, tp = lax.axis_size("sp"), lax.axis_size("tp")
    inner = INNER if sp % INNER == 0 else 1
    near = [[g * inner + i for i in range(inner)] for g in range(sp // inner)]
    far = [[g * inner + i for g in range(sp // inner)] for i in range(inner)]
    hidden = w_gate.shape[1] // inner

    q, y, ps = recurrence(r, k, v, dw, lw)
    ps_all = lax.all_gather(ps, "sp")

    def by_columns(w):
        w = lax.all_to_all(
            w, "sp", split_axis=1, concat_axis=0, axis_index_groups=near, tiled=True
        )
        return lax.all_gather(w, "sp", axis_index_groups=far, axis=0, tiled=False)

    g_all, u_all = by_columns(w_gate), by_columns(w_up)
    g_all = g_all.reshape(-1, hidden)
    u_all = u_all.reshape(-1, hidden)
    d_part = lax.all_to_all(
        w_down, "sp", split_axis=0, concat_axis=1, axis_index_groups=near, tiled=True
    )
    d_all = lax.all_gather(d_part, "sp", axis_index_groups=far, axis=1, tiled=True)

    index = lax.axis_index("sp").astype(jnp.int32).reshape(1)
    part = join(
        index, ps_all, q, y, r, k, v, gate, tw.reshape(1, -1), hg.reshape(1, -1), w_out
    )
    own_rows = steps // tp
    start = lax.axis_index("tp") * own_rows
    mix = lax.all_to_all(part.reshape(tp, own_rows, -1), "tp", 0, 0)
    mix = jnp.sum(mix.astype(jnp.float32), axis=0).astype(jnp.bfloat16).astype(jnp.float32)
    mine = lax.dynamic_slice_in_dim(residual, start, own_rows, 0)
    after = (mine.astype(jnp.float32) + mix).astype(jnp.bfloat16)
    normed = lax.all_gather(rms_scale(after, gain), "tp", axis=0, tiled=True)
    normed = lax.all_gather(normed, "sp", axis_index_groups=near, axis=0, tiled=True)
    g = jnp.dot(normed, g_all, preferred_element_type=jnp.float32)
    u = jnp.dot(normed, u_all, preferred_element_type=jnp.float32)
    h = (jax.nn.silu(g) * u).astype(jnp.bfloat16)
    down = jnp.dot(h, d_all, preferred_element_type=jnp.float32).astype(jnp.bfloat16)
    down = down.reshape(inner, tp, own_rows, -1)
    down = lax.all_to_all(down, "sp", 0, 0, axis_index_groups=near)
    down = jnp.sum(down.astype(jnp.float32), axis=0).astype(jnp.bfloat16)
    down = lax.all_to_all(down, "tp", 0, 0)
    down = jnp.sum(down.astype(jnp.float32), axis=0)
    return (after.astype(jnp.float32) + down).astype(jnp.bfloat16)


def solution(mesh):
    split_both = P("sp", "tp")
    placed = (split_both,) * 6 + (
        P("tp", None),
        P("tp"),
        P("tp", None),
        P("sp", None),
        P(),
        split_both,
        split_both,
        P("tp", "sp"),
    )
    return jax.shard_map(
        per_device, mesh=mesh, in_specs=placed, out_specs=P(("sp", "tp"), None), check_vma=False
    )
```

time: 1510 us -> 382 us (0.25); the launches traced: 1480 us -> 376 us
  matrix products: 487 us -> 17.4 us
  local copies, waits for them, and re-layouts: 384 us -> 4.65 us
  waiting for transfers between devices: 448 us -> 224 us
  other arithmetic: 141 us -> 3.24 us
  blocking collectives: 2.58 us -> 86.8 us
  Pallas kernels: 0 us -> 27.3 us
    dot_general x96 -> x2, matrix products: 487 us -> 17.4 us  [the longest x1 10.5 us: per_device(): jnp.dot(h, d_all, preferred_element_type=jnp.float32).astype(jnp.bfloat16)]
    all_gather x5, waiting for transfers between devices: 428 us -> 224 us  [the longest x2 67.4 us: by_columns(): return lax.all_gather(w, 'sp', axis_index_groups=far, axis=0, tiled=False)]
    pad x10 -> x0, local copies, waits for them, and re-layouts: 144 us -> none  [per_device(): inclusive = lax.associative_scan(compose, (block_prod, block_state), axis=0)]
    add x23 -> x0, other arithmetic: 123 us -> none  [the longest x16 106 us: advance(): memory * decay_t[:, :, None, :]]
    dynamic_update_slice x32 -> x0, local copies, waits for them, and re-layouts: 88.3 us -> none  [per_device(): lax.scan(advance, (block_eye, jnp.zeros_like(block_eye)), series)]
    all_to_all x0 -> x6, blocking collectives: none -> 84.2 us  [the longest x1 37.6 us: per_device(): down = lax.all_to_all(down, 'sp', 0, 0, axis_index_groups=near)]
    mul x37 -> x0, local copies, waits for them, and re-layouts: 29.8 us -> none  [the longest x16 13.4 us: advance(): shifted[..., None] * insert_t[:, :, None, :]]
    dynamic_slice x46 -> x0, local copies, waits for them, and re-layouts: 29.8 us -> none  [the longest x30 16.5 us: turn(): longer = join(running, jax.tree.map(lambda part: part[position], pieces))]
  transfers between devices with their start and end apart: 7 -> 5, of which waited for: 6 -> 5; matrix products, arithmetic and copies ran while one was open for 10% -> 3% of each run, Pallas kernels for 0% -> 2%
where the time goes in v1:
time: 382 us; the launch traced here: 376 us
  waiting for transfers between devices  224 us (59%)
  blocking collectives  86.8 us (23%)
  Pallas kernels  27.3 us (7%)
  matrix products  17.4 us (5%)
  between operations  13.2 us (3%)
  local copies, waits for them, and re-layouts  4.65 us (1%)
    all_gather x2, waiting for transfers between devices, by_columns(): return lax.all_gather(w, 'sp', axis_index_groups=far, axis=0, tiled=False)  67.4 us
    all_gather x1, waiting for transfers between devices, per_device(): ps_all = lax.all_gather(ps, 'sp')  62.3 us
    all_gather x1, waiting for transfers between devices, per_device(): lax.all_gather(d_part, 'sp', axis_index_groups=far, axis=1, tiled=True)  48.2 us
    all_gather x1, waiting for transfers between devices, per_device(): lax.all_gather(normed, 'sp', axis_index_groups=near, axis=0, tiled=True)  45.6 us
    all_to_all x1, blocking collectives, per_device(): down = lax.all_to_all(down, 'sp', 0, 0, axis_index_groups=near)  37.6 us
    all_to_all x2, blocking collectives, by_columns(): lax.all_to_all(w, 'sp', split_axis=1, concat_axis=0, axis_index_groups=ne...  21.1 us
    pallas_call x1, Pallas kernels, recurrence(): pl.pallas_call(local_kernel, grid=(pairs,), in_specs=[cols] * 5, out_spec...  19.5 us
    all_to_all x1, blocking collectives, per_device(): lax.all_to_all(w_down, 'sp', split_axis=0, concat_axis=1, axis_index_grou...  11.2 us
  transfers between devices with their start and end apart: 5, of which 5 were waited for; matrix products, arithmetic and copies ran while one was open for 3% of the time, Pallas kernels for 2%

profile of v1, /device:TPU:15, one launch (start us, length us, event | category | flops | bytes accessed | tf_op | source)
XLA Modules:
  0.0 376.4 jit_solution(2663676046423373794)
XLA Ops:
  6.5 19.5 %local_part.1 = (f32[192,512]{1,0:T(8,128)}, f32[192,512]{1,0:T(8,128)}, f32[4,2,64,128]{3,2,1,0:T(8,128)}) custom-call(bf16[192,512]{1,0:T(8,128)(2,1)} %r_ref.3, bf16[192,512]{1,0:T(8,128)(2,1)} %k_ref.3, bf16[192,512]{1,0:T(8,128)(2,1)} %v_ref.3, f32[192,512]{1,0:T(8,128)} %dw_ref.1, f32[192,512]{1,0:T(8,128)} %lw_ref.1), custom_call_target="tpu_custom_call" | custom-call | flops 20000000000 | bytes 4000000 | tf_op jit(solution)/shard_map/local_part/pallas_call | solution.py:175
  26.2 0.3 copy.25
  26.5 10.8 %all_to_all.66 = bf16[128,4,640]{0,2,1:T(8,128)(2,1)S(1)} all-to-all(bf16[128,4,640]{0,2,1:T(8,128)(2,1)S(1)} %bitcast.27), channel_id=1, replica_groups={{0,2,4,6},{8,10,12,14},{16,18,20,22},{24,26,28,30},{1,3,5,7},{9,11,13,1..., dimensions={1} | all-to-all | bytes 1310720 | tf_op jit(solution)/shard_map/all_to_all | solution.py:224
  37.3 1.1 copy.26
  38.5 0.7 reshape.42.tw_ref
  39.1 62.3 %all-gather.15.cloned.1.call-done = f32[64,2,64,128]{3,2,1,0:T(8,128)} async-done(((f32[4,2,64,128]{3,2,1,0:T(8,128)}), f32[64,2,64,128]{3,2,1,0:T(8,128)}) %all-gather.15.cloned.1.call-update) | async-done | bytes 4194320 | tf_op jit(solution)/shard_map/all_gather | solution.py:221
  101.4 7.8 %join_part.1 = bf16[192,2048]{1,0:T(8,128)(2,1)} custom-call(s32[1]{0:T(128)} %bitcast.i_ref, f32[16,4,2,64,128]{4,3,2,1,0:T(8,128)} %bitcast.32, f32[192,512]{1,0:T(8,128)} %get-tuple-element.9.q_ref, f32[192,512]{1,0:T(8,128)} %get-tuple-element.10.y_ref, bf16[192,512]{1,0:T(8,128)(2,1)} %r_ref.3, bf16[192,512]{1,0:T(8,128)(2,1)} %k_ref.3, ...), custom_call_target="tpu_custom_call" | custom-call | flops 10000000000 | bytes 8000000 | tf_op jit(solution)/shard_map/join_part/pallas_call | solution.py:194
  109.2 7.1 %all_to_all.67 = bf16[2,96,2048]{2,1,0:T(8,128)(2,1)S(1)} all-to-all(bf16[2,96,2048]{2,1,0:T(8,128)(2,1)} %bitcast.30), channel_id=1, replica_groups=mesh['sp'=16,'tp'=2] {'tp'}, dimensions={0} | all-to-all | bytes 1572864 | tf_op jit(solution)/shard_map/all_to_all | solution.py:243
  116.9 2.6 all_gather.29
  119.6 11.2 %all_to_all.68 = bf16[4,640,128]{2,1,0:T(8,128)(2,1)S(1)} all-to-all(bf16[4,640,128]{2,1,0:T(8,128)(2,1)S(1)} %bitcast.31), channel_id=1, replica_groups={{0,2,4,6},{8,10,12,14},{16,18,20,22},{24,26,28,30},{1,3,5,7},{9,11,13,1..., dimensions={0} | all-to-all | bytes 1310720 | tf_op jit(solution)/shard_map/all_to_all | solution.py:232
  130.8 1.1 copy.29
  132.0 0.3 copy.27
  132.3 10.3 %all_to_all.69 = bf16[128,4,640]{0,2,1:T(8,128)(2,1)S(1)} all-to-all(bf16[128,4,640]{0,2,1:T(8,128)(2,1)S(1)} %bitcast.29), channel_id=1, replica_groups={{0,2,4,6},{8,10,12,14},{16,18,20,22},{24,26,28,30},{1,3,5,7},{9,11,13,1..., dimensions={1} | all-to-all | bytes 1310720 | tf_op jit(solution)/shard_map/all_to_all | solution.py:224
  142.6 1.1 copy.28
  143.8 12.5 %all-gather.9.cloned.1.call-done = bf16[4,512,640]{2,1,0:T(8,128)(2,1)} async-done(((bf16[1,512,640]{2,1,0:T(8,128)(2,1)}), bf16[4,512,640]{2,1,0:T(8,128)(2,1)}) %all-gather.9.cloned.1.call-update) | async-done | bytes 2621456 | tf_op jit(solution)/shard_map/all_gather | solution.py:227
  156.2 45.6 %all-gather.7.cloned.1.call-done = bf16[768,2048]{1,0:T(8,128)(2,1)} async-done(((bf16[192,2048]{1,0:T(8,128)(2,1)}), bf16[768,2048]{1,0:T(8,128)(2,1)}) %all-gather.7.cloned.1.call-update) | async-done | bytes 3145744 | tf_op jit(solution)/shard_map/all_gather | solution.py:248
  201.8 6.8 %fusion.5 = f32[768,640]{1,0:T(8,128)} fusion(bf16[768,2048]{1,0:T(8,128)(2,1)} %all-gather.7.cloned.1.call-done, bf16[2048,640]{1,0:T(8,128)(2,1)} %bitcast.33), kind=kOutput, calls=%fused_computation.13 | convolution fusion | flops 2013265920 | bytes 7733248 | tf_op jit(solution)/shard_map/dot_general | solution.py:249
  208.7 48.2 %all-gather.13.cloned.1.call-done = bf16[640,2048]{0,1:T(8,128)(2,1)} async-done(((bf16[640,512]{0,1:T(8,128)(2,1)}), bf16[640,2048]{0,1:T(8,128)(2,1)}) %all-gather.13.cloned.1.call-update) | async-done | bytes 2621456 | tf_op jit(solution)/shard_map/all_gather | solution.py:235
  256.9 55.0 %all-gather.11.cloned.1.call-done = bf16[4,512,640]{2,1,0:T(8,128)(2,1)} async-done(((bf16[1,512,640]{2,1,0:T(8,128)(2,1)}), bf16[4,512,640]{2,1,0:T(8,128)(2,1)}) %all-gather.11.cloned.1.call-update) | async-done | bytes 2621456 | tf_op jit(solution)/shard_map/all_gather | solution.py:227
  311.9 10.5 %convolution_convert_fusion = bf16[768,2048]{1,0:T(8,128)(2,1)} fusion(bf16[640,2048]{0,1:T(8,128)(2,1)} %all-gather.13.cloned.1.call-done, f32[768,640]{1,0:T(8,128)} %fusion.5, bf16[768,2048]{1,0:T(8,128)(2,1)S(1)} %copy-done.6, bf16[2048,640]{1,0:T(8,128)(2,1)} %bitcast.34), kind=kOutput, calls=%fused_computation | convolution fusion | flops 4031053824 | bytes 13500416 | tf_op jit(solution)/shard_map/dot_general | solution.py:252
  322.4 37.6 %all_to_all.70 = bf16[4,2,96,2048]{3,2,1,0:T(8,128)(2,1)S(1)} all-to-all(bf16[4,2,96,2048]{3,2,1,0:T(8,128)(2,1)} %bitcast.21), channel_id=1, replica_groups={{0,2,4,6},{8,10,12,14},{16,18,20,22},{24,26,28,30},{1,3,5,7},{9,11,13,1..., dimensions={0} | all-to-all | bytes 6291456 | tf_op jit(solution)/shard_map/all_to_all | solution.py:254
  360.1 1.7 reduce_sum.44
  361.8 7.2 %all_to_all.71 = bf16[2,96,2048]{2,1,0:T(8,128)(2,1)S(1)} all-to-all(bf16[2,96,2048]{2,1,0:T(8,128)(2,1)} %reduce_sum.44), channel_id=1, replica_groups=mesh['sp'=16,'tp'=2] {'tp'}, dimensions={0} | all-to-all | bytes 1572864 | tf_op jit(solution)/shard_map/all_to_all | solution.py:256
  369.1 0.8 fusion.3
  (29 shorter events, 1.0 us)
Async XLA Ops:
  6.5 19.6 %copy-start = (bf16[128,2560]{1,0:T(8,128)(2,1)S(1)}, bf16[128,2560]{1,0:T(8,128)(2,1)}, u32[]{:S(2)}) copy-start(bf16[128,2560]{1,0:T(8,128)(2,1)} %param.25) | copy-start | bytes 1966084
  6.5 94.9 %all-gather.15.cloned.1.call-start = ((), (), s32[]{:S(2)}) async-start(), calls=%async_computation.10 | async-start | bytes 4456448 | tf_op jit(solution)/shard_map/all_gather | solution.py:221
  26.1 12.4 %copy-start.5 = (f32[8,64]{1,0:T(8,128)S(1)}, f32[8,64]{1,0:T(8,128)}, u32[]{:S(2)}) copy-start(f32[8,64]{1,0:T(8,128)} %param.20) | copy-start | bytes 6148
  26.1 130.1 %all-gather.9.cloned.1.call-start = ((), (), s32[]{:S(2)}) async-start(), calls=%async_computation.7 | async-start | bytes 3276800 | tf_op jit(solution)/shard_map/all_gather | solution.py:227
  38.4 163.4 %all-gather.7.cloned.1.call-start = ((), (), s32[]{:S(2)}) async-start(), calls=%async_computation.6 | async-start | bytes 3932160 | tf_op jit(solution)/shard_map/all_gather | solution.py:248
  109.1 7.3 %copy-start.3 = (bf16[192,2048]{1,0:T(8,128)(2,1)S(1)}, bf16[192,2048]{1,0:T(8,128)(2,1)}, u32[]{:S(2)}) copy-start(bf16[192,2048]{1,0:T(8,128)(2,1)} %param.23) | copy-start | bytes 2359300
  109.2 7.6 %copy-start.4 = (f32[2048]{0:T(1024)S(1)}, f32[2048]{0:T(1024)}, u32[]{:S(2)}) copy-start(f32[2048]{0:T(1024)} %param.24) | copy-start | bytes 24580
  116.3 3.3 copy-start.1
  116.9 15.1 %copy-start.2 = (bf16[128,2560]{1,0:T(8,128)(2,1)S(1)}, bf16[128,2560]{1,0:T(8,128)(2,1)}, u32[]{:S(2)}) copy-start(bf16[128,2560]{1,0:T(8,128)(2,1)} %param.26) | copy-start | bytes 1966084
  119.6 137.4 %all-gather.13.cloned.1.call-start = ((), (), s32[]{:S(2)}) async-start(), calls=%async_computation.9 | async-start | bytes 3276800 | tf_op jit(solution)/shard_map/all_gather | solution.py:235
  131.9 180.0 %all-gather.11.cloned.1.call-start = ((), (), s32[]{:S(2)}) async-start(), calls=%async_computation.8 | async-start | bytes 3276800 | tf_op jit(solution)/shard_map/all_gather | solution.py:227
  201.8 110.0 %copy-start.6 = (bf16[768,2048]{1,0:T(8,128)(2,1)S(1)}, bf16[768,2048]{1,0:T(8,128)(2,1)}, u32[]{:S(2)}) copy-start(bf16[768,2048]{1,0:T(8,128)(2,1)} %all-gather.7.cloned.1.call-done) | copy-start | bytes 9437188
Sparse Core Ops, SparseCore 0:
  26.2 75.1 all-gather.14
  103.0 53.2 all-gather.8
  158.1 43.7 all-gather.6
  203.3 53.6 all-gather.12
  258.3 53.5 all-gather.10

commit v2 on v1

--- a/solution.py
+++ b/solution.py
@@ -15,6 +15,7 @@
 NT = (((1,), (1,)), ((), ()))
 TN = (((0,), (0,)), ((), ()))
 INNER = 4
+MESH = pl.DeviceIdType.MESH
 
 
 def split(x):
@@ -203,6 +204,96 @@
     )(index, ps, q, y, r, k, v, gate, tw, hg, w)
 
 
+def weights_kernel(inner, outer, g_ref, u_ref, d_ref, g_out, u_out, d_out, s1, r1, s2, r2, own_sem):
+    me = lax.axis_index("sp")
+    a, b = me // outer, me % outer
+    wide = g_out.shape[2]
+
+    def peer_a(step):
+        return (a + step + inner) % inner * outer + b
+
+    def peer_b(step):
+        return a * outer + (b + step + outer) % outer
+
+    barrier = pltpu.get_barrier_semaphore()
+    for step in range(1, inner):
+        pl.semaphore_signal(barrier, inc=1, device_id={"sp": peer_a(step)}, device_id_type=MESH)
+    for step in range(1, outer):
+        pl.semaphore_signal(barrier, inc=1, device_id={"sp": peer_b(step)}, device_id_type=MESH)
+    pl.semaphore_wait(barrier, inner - 1 + outer - 1)
+    outs = (g_out, u_out, d_out)
+
+    def cut(which, part):
+        at = pl.ds(pl.multiple_of(part * wide, 128), wide)
+        return d_ref.at[at, :] if which == 2 else (g_ref, u_ref)[which].at[:, at]
+
+    def send(src, dst, send_sem, recv_sem, target):
+        copy = pltpu.make_async_remote_copy(
+            src_ref=src,
+            dst_ref=dst,
+            send_sem=send_sem,
+            recv_sem=recv_sem,
+            device_id={"sp": target},
+            device_id_type=MESH,
+        )
+        copy.start()
+        return copy
+
+    waits, early = [], {}
+    for step in range(1, inner):
+        for w in range(3):
+            early[step, w] = send(
+                cut(w, (a + step) % inner), outs[w].at[me], s1.at[step, w], r1.at[step, w], peer_a(step)
+            )
+    for w in range(3):
+        copy = pltpu.make_async_copy(cut(w, a), outs[w].at[me], own_sem.at[w])
+        copy.start()
+        waits.append(copy)
+    for step in range(inner):
+        slot = peer_a(-step)
+        for w in range(3):
+            if step:
+                early[step, w].wait()
+            src = outs[w].at[slot] if step else cut(w, a)
+            for hop in range(1, outer):
+                waits.append(
+                    send(src, outs[w].at[slot], s2.at[step, hop, w], r2.at[step, hop, w], peer_b(hop))
+                )
+    for copy in waits:
+        copy.wait()
+
+
+def spread_weights(inner, w_gate, w_up, w_down):
+    sp = lax.axis_size("sp")
+    outer = sp // inner
+    rows, cols = w_gate.shape
+    wide = cols // inner
+    vmem = pl.BlockSpec(memory_space=pltpu.VMEM)
+    wide_shape = jax.ShapeDtypeStruct((sp, rows, wide), w_gate.dtype)
+    tall_shape = jax.ShapeDtypeStruct((sp, wide, w_down.shape[1]), w_down.dtype)
+    sems = pltpu.SemaphoreType.DMA
+    return pl.pallas_call(
+        functools.partial(weights_kernel, inner, outer),
+        in_specs=[vmem] * 3,
+        out_specs=[vmem] * 3,
+        out_shape=[wide_shape, wide_shape, tall_shape],
+        scratch_shapes=[
+            sems((inner, 3)),
+            sems((inner, 3)),
+            sems((inner, outer, 3)),
+            sems((inner, outer, 3)),
+            sems((3,)),
+        ],
+        compiler_params=pltpu.CompilerParams(
+            collective_id=0, has_side_effects=True, vmem_limit_bytes=40 * 1024 * 1024
+        ),
+        cost_estimate=pl.CostEstimate(
+            flops=50_000_000_000, bytes_accessed=100_000_000, transcendentals=0
+        ),
+        name="spread_weights",
+    )(w_gate, w_up, w_down)
+
+
 def rms_scale(rows, gain):
     x = rows.astype(jnp.float32)
     factor = lax.rsqrt(jnp.mean(x * x, axis=-1, keepdims=True) + NORM_EPS)
@@ -212,27 +303,20 @@
 def per_device(r, k, v, dw, lw, gate, tw, hg, w_out, residual, gain, w_gate, w_up, w_down):
     steps = r.shape[0]
     sp, tp = lax.axis_size("sp"), lax.axis_size("tp")
-    inner = INNER if sp % INNER == 0 else 1
-    near = [[g * inner + i for i in range(inner)] for g in range(sp // inner)]
-    far = [[g * inner + i for g in range(sp // inner)] for i in range(inner)]
+    fits = sp % INNER == 0 and w_gate.shape[1] % (INNER * LANES) == 0
+    inner = INNER if fits else 1
+    outer = sp // inner
+    near = [[i * outer + j for i in range(inner)] for j in range(outer)]
     hidden = w_gate.shape[1] // inner
 
     q, y, ps = recurrence(r, k, v, dw, lw)
     ps_all = lax.all_gather(ps, "sp")
 
-    def by_columns(w):
-        w = lax.all_to_all(
-            w, "sp", split_axis=1, concat_axis=0, axis_index_groups=near, tiled=True
-        )
-        return lax.all_gather(w, "sp", axis_index_groups=far, axis=0, tiled=False)
-
-    g_all, u_all = by_columns(w_gate), by_columns(w_up)
+    w_gate, w_up, w_down, q = lax.optimization_barrier((w_gate, w_up, w_down, q))
+    g_all, u_all, d_all = spread_weights(inner, w_gate, w_up, w_down)
     g_all = g_all.reshape(-1, hidden)
     u_all = u_all.reshape(-1, hidden)
-    d_part = lax.all_to_all(
-        w_down, "sp", split_axis=0, concat_axis=1, axis_index_groups=near, tiled=True
-    )
-    d_all = lax.all_gather(d_part, "sp", axis_index_groups=far, axis=1, tiled=True)
+    d_all = jnp.moveaxis(d_all, 0, 1).reshape(hidden, -1)
 
     index = lax.axis_index("sp").astype(jnp.int32).reshape(1)
     part = join(

time: 382 us -> 354 us (0.927)
  waiting for transfers between devices: 224 us -> 74.1 us
  Pallas kernels: 27.3 us -> 137 us
  blocking collectives: 86.8 us -> 93.7 us
  local copies, waits for them, and re-layouts: 4.65 us -> 9.27 us
    all_gather x3 -> x0, waiting for transfers between devices: 116 us -> none  [the longest x2 67.4 us: by_columns(): return lax.all_gather(w, 'sp', axis_index_groups=far, axis=0, tiled=False)]
    pallas_call x0 -> x1, Pallas kernels: none -> 110 us  [spread_weights(): pl.pallas_call(functools.partial(weights_kernel, inner, outer), in_specs=...]
    all_gather x1, waiting for transfers between devices: 45.6 us -> 0.01 us  [per_device(): lax.all_gather(normed, 'sp', axis_index_groups=near, axis=0, tiled=True)]
    all_to_all x1, blocking collectives: 37.6 us -> 76.2 us  [per_device(): down = lax.all_to_all(down, 'sp', 0, 0, axis_index_groups=near)]
    all_to_all x3 -> x0, blocking collectives: 32.3 us -> none  [the longest x2 21.1 us: by_columns(): lax.all_to_all(w, 'sp', split_axis=1, concat_axis=0, axis_index_groups=ne...]
    all_gather x1, waiting for transfers between devices: 62.3 us -> 74 us  [per_device(): ps_all = lax.all_gather(ps, 'sp')]
    unnamed x16 -> x22, local copies, waits for them, and re-layouts: 0.69 us -> 5.98 us
  transfers between devices with their start and end apart: 5 -> 2, of which waited for: 5 -> 1; matrix products, arithmetic and copies ran while one was open for 3% -> 1% of each run, Pallas kernels for 2% -> 32%
where the time goes in v2:
time: 354 us; the launch traced here: 347 us
  Pallas kernels  137 us (39%)
  blocking collectives  93.7 us (26%)
  waiting for transfers between devices  74.1 us (21%)
  matrix products  16.6 us (5%)
  between operations  13.5 us (4%)
  local copies, waits for them, and re-layouts  9.27 us (3%)
    pallas_call x1, Pallas kernels, spread_weights(): pl.pallas_call(functools.partial(weights_kernel, inner, outer), in_specs=...  110 us
    all_to_all x1, blocking collectives, per_device(): down = lax.all_to_all(down, 'sp', 0, 0, axis_index_groups=near)  76.2 us
    all_gather x1, waiting for transfers between devices, per_device(): ps_all = lax.all_gather(ps, 'sp')  74 us
    pallas_call x1, Pallas kernels, recurrence(): pl.pallas_call(local_kernel, grid=(pairs,), in_specs=[cols] * 5, out_spec...  19.4 us
    dot_general x1, matrix products, per_device(): jnp.dot(h, d_all, preferred_element_type=jnp.float32).astype(jnp.bfloat16)  9.78 us
    all_to_all x1, blocking collectives, per_device(): down = lax.all_to_all(down, 'tp', 0, 0)  7.96 us
    pallas_call x1, Pallas kernels, join(): pl.pallas_call(join_kernel, in_specs=[pl.BlockSpec(memory_space=pltpu.SME...  7.72 us
  transfers between devices with their start and end apart: 2, of which 1 were waited for; matrix products, arithmetic and copies ran while one was open for 1% of the time, Pallas kernels for 32%

profile of v2, /device:TPU:15, one launch (start us, length us, event | category | flops | bytes accessed | tf_op | source)
XLA Modules:
  0.0 347.3 jit_solution(15325246192350318770)
XLA Ops:
  6.5 19.4 %local_part.1 = (f32[192,512]{1,0:T(8,128)}, f32[192,512]{1,0:T(8,128)}, f32[4,2,64,128]{3,2,1,0:T(8,128)}) custom-call(bf16[192,512]{1,0:T(8,128)(2,1)} %r_ref.3, bf16[192,512]{1,0:T(8,128)(2,1)} %k_ref.3, bf16[192,512]{1,0:T(8,128)(2,1)} %v_ref.3, f32[192,512]{1,0:T(8,128)} %dw_ref.1, f32[192,512]{1,0:T(8,128)} %lw_ref.1), custom_call_target="tpu_custom_call" | custom-call | flops 20000000000 | bytes 4000000 | tf_op jit(solution)/shard_map/local_part/pallas_call | solution.py:176
  26.0 0.0 all-gather.4.cloned.1.call-start
  26.1 0.7 reshape.34.tw_ref
  26.7 74.0 %all-gather.6.cloned.1.call-done = f32[64,2,64,128]{3,2,1,0:T(8,128)} async-done(((f32[4,2,64,128]{3,2,1,0:T(8,128)}), f32[64,2,64,128]{3,2,1,0:T(8,128)}) %all-gather.6.cloned.1.call-update) | async-done | bytes 4194320 | tf_op jit(solution)/shard_map/all_gather | solution.py:313
  100.8 7.7 %join_part.1 = bf16[192,2048]{1,0:T(8,128)(2,1)} custom-call(s32[1]{0:T(128)} %bitcast.i_ref, f32[16,4,2,64,128]{4,3,2,1,0:T(8,128)} %bitcast.20, f32[192,512]{1,0:T(8,128)} %get-tuple-element.17.q_ref, f32[192,512]{1,0:T(8,128)} %get-tuple-element.18.y_ref, bf16[192,512]{1,0:T(8,128)(2,1)} %r_ref.3, bf16[192,512]{1,0:T(8,128)(2,1)} %k_ref.3, ...), custom_call_target="tpu_custom_call" | custom-call | flops 10000000000 | bytes 8000000 | tf_op jit(solution)/shard_map/join_part/pallas_call | solution.py:195
  108.5 7.1 %all_to_all.15 = bf16[2,96,2048]{2,1,0:T(8,128)(2,1)S(1)} all-to-all(bf16[2,96,2048]{2,1,0:T(8,128)(2,1)} %bitcast.19), channel_id=1, replica_groups=mesh['sp'=16,'tp'=2] {'tp'}, dimensions={0} | all-to-all | bytes 1572864 | tf_op jit(solution)/shard_map/all_to_all | solution.py:327
  115.5 0.2 reduce_sum.42
  115.7 0.2 fusion
  116.0 0.7 copy-done.6
  116.7 0.2 fusion.2
  116.9 2.5 all_gather.14
  119.5 1.1 copy-done.1
  120.5 1.1 copy-done.2
  121.6 109.7 %spread_weights.1 = (bf16[16,128,640]{2,1,0:T(8,128)(2,1)S(1)}, bf16[16,128,640]{2,1,0:T(8,128)(2,1)S(1)}, bf16[16,640,128]{2,1,0:T(8,128)(2,1)S(1)}) custom-call(bf16[128,2560]{1,0:T(8,128)(2,1)S(1)} %copy-done, bf16[128,2560]{1,0:T(8,128)(2,1)S(1)} %copy-done.1, bf16[2560,128]{1,0:T(8,128)(2,1)S(1)} %copy-done.2), custom_call_target="tpu_custom_call" | custom-call | flops 49999998976 | bytes 100000000 | tf_op jit(solution)/shard_map/spread_weights/pallas_call | solution.py:275
  231.3 1.5 copy-done.3
  232.8 1.5 copy-done.5
  234.4 2.6 copy.17
  237.0 6.8 %fusion.5 = f32[768,640]{1,0:T(8,128)} fusion(bf16[768,2048]{1,0:T(8,128)(2,1)} %all-gather.4.cloned.1.call-done, bf16[2048,640]{1,0:T(8,128)(2,1)} %bitcast.16), kind=kOutput, calls=%fused_computation.13 | convolution fusion | flops 2013265920 | bytes 7733248 | tf_op jit(solution)/shard_map/dot_general | solution.py:333
  243.8 9.8 %convolution_convert_fusion = bf16[768,2048]{1,0:T(8,128)(2,1)} fusion(bf16[640,2048]{0,1:T(8,128)(2,1)} %bitcast.18, f32[768,640]{1,0:T(8,128)} %fusion.5, bf16[768,2048]{1,0:T(8,128)(2,1)} %all-gather.4.cloned.1.call-done, bf16[2048,640]{1,0:T(8,128)(2,1)S(1)} %bitcast.15), kind=kOutput, calls=%fused_computation | convolution fusion | flops 4031053824 | bytes 13500416 | tf_op jit(solution)/shard_map/dot_general | solution.py:336
  253.6 76.2 %all_to_all.16 = bf16[4,2,96,2048]{3,2,1,0:T(8,128)(2,1)S(1)} all-to-all(bf16[4,2,96,2048]{3,2,1,0:T(8,128)(2,1)} %bitcast.17), channel_id=1, replica_groups={{0,8,16,24},{2,10,18,26},{4,12,20,28},{6,14,22,30},{1,9,17,25},{3,11,19..., dimensions={0} | all-to-all | bytes 6291456 | tf_op jit(solution)/shard_map/all_to_all | solution.py:338
  329.8 1.7 reduce_sum.44
  331.5 8.0 %all_to_all.17 = bf16[2,96,2048]{2,1,0:T(8,128)(2,1)S(1)} all-to-all(bf16[2,96,2048]{2,1,0:T(8,128)(2,1)} %reduce_sum.44), channel_id=1, replica_groups=mesh['sp'=16,'tp'=2] {'tp'}, dimensions={0} | all-to-all | bytes 1572864 | tf_op jit(solution)/shard_map/all_to_all | solution.py:340
  339.5 0.1 convert_reduce_fusion
  339.6 0.8 fusion.3
  (22 shorter events, 0.1 us)
Async XLA Ops:
  6.5 19.5 %copy-start.10 = (f32[8,64]{1,0:T(8,128)S(1)}, f32[8,64]{1,0:T(8,128)}, u32[]{:S(2)}) copy-start(f32[8,64]{1,0:T(8,128)} %param.20) | copy-start | bytes 6148
  6.5 94.2 %all-gather.6.cloned.1.call-start = ((), (), s32[]{:S(2)}) async-start(), calls=%async_computation.4 | async-start | bytes 4456448 | tf_op jit(solution)/shard_map/all_gather | solution.py:313
  26.0 211.0 %all-gather.4.cloned.1.call-start = ((), (), s32[]{:S(2)}) async-start(), calls=%async_computation.3 | async-start | bytes 3932160 | tf_op jit(solution)/shard_map/all_gather | solution.py:332
  108.5 7.3 %copy-start.8 = (bf16[192,2048]{1,0:T(8,128)(2,1)S(1)}, bf16[192,2048]{1,0:T(8,128)(2,1)}, u32[]{:S(2)}) copy-start(bf16[192,2048]{1,0:T(8,128)(2,1)} %param.23) | copy-start | bytes 2359300
  108.5 8.3 %copy-start.9 = (f32[2048]{0:T(1024)S(1)}, f32[2048]{0:T(1024)}, u32[]{:S(2)}) copy-start(f32[2048]{0:T(1024)} %param.24) | copy-start | bytes 24580
  115.5 3.9 %copy-start = (bf16[128,2560]{1,0:T(8,128)(2,1)S(1)}, bf16[128,2560]{1,0:T(8,128)(2,1)}, u32[]{:S(2)}) copy-start(bf16[128,2560]{1,0:T(8,128)(2,1)} %g_ref.2) | copy-start | bytes 1966084
  116.0 0.7 copy-start.6
  119.4 1.1 copy-start.1
  120.5 1.1 copy-start.2
  231.3 1.5 copy-start.3
  232.8 1.5 copy-start.5
  237.0 6.8 %copy-start.4 = (bf16[16,128,640]{2,1,0:T(8,128)(2,1)S(1)}, bf16[16,128,640]{2,1,0:T(8,128)(2,1)}, u32[]{:S(2)}) copy-start(bf16[16,128,640]{2,1,0:T(8,128)(2,1)} %copy-done.3) | copy-start | bytes 7864324
  329.8 9.8 %copy-start.7 = (bf16[96,2048]{1,0:T(8,128)(2,1)S(1)}, bf16[96,2048]{1,0:T(8,128)(2,1)}, u32[]{:S(2)}) copy-start(bf16[96,2048]{1,0:T(8,128)(2,1)} %copy-done.6) | copy-start | bytes 1179652
Sparse Core Ops, SparseCore 0:
  26.1 74.5 all-gather.5
  119.6 98.3 all-gather.3

commit v3 on v2

--- a/solution.py
+++ b/solution.py
@@ -294,6 +294,89 @@
     )(w_gate, w_up, w_down)
 
 
+def rows_kernel(inner, tp, scatter, x_ref, out_ref, s1, r1, s2, r2, own_sem):
+    sp_at, t = lax.axis_index("sp"), lax.axis_index("tp")
+    outer = lax.axis_size("sp") // inner
+    a, b = sp_at // outer, sp_at % outer
+    barrier = pltpu.get_barrier_semaphore()
+
+    def at(step):
+        return (a + step + inner) % inner
+
+    def far(step):
+        return {"sp": at(step) * outer + b, "tp": t}
+
+    def near(step):
+        return {"sp": sp_at, "tp": (t + step) % tp}
+
+    near_steps = () if scatter else range(1, tp)
+    for step in range(1, inner):
+        pl.semaphore_signal(barrier, inc=1, device_id=far(step), device_id_type=MESH)
+    for step in near_steps:
+        pl.semaphore_signal(barrier, inc=1, device_id=near(step), device_id_type=MESH)
+    pl.semaphore_wait(barrier, inner - 1 + len(near_steps))
+
+    def send(src, dst, send_sem, recv_sem, target):
+        copy = pltpu.make_async_remote_copy(
+            src_ref=src,
+            dst_ref=dst,
+            send_sem=send_sem,
+            recv_sem=recv_sem,
+            device_id=target,
+            device_id_type=MESH,
+        )
+        copy.start()
+        return copy
+
+    def slot(which):
+        return out_ref.at[which] if scatter else out_ref.at[t, which]
+
+    early = {}
+    for step in range(1, inner):
+        src = x_ref.at[at(step)] if scatter else x_ref
+        early[step] = send(src, slot(a), s1.at[step], r1.at[step], far(step))
+    own = pltpu.make_async_copy(x_ref.at[a] if scatter else x_ref, slot(a), own_sem)
+    own.start()
+    waits = [own]
+    for step in range(inner):
+        if step:
+            early[step].wait()
+        for hop in near_steps:
+            src = slot(at(-step)) if step else x_ref
+            waits.append(
+                send(src, slot(at(-step)), s2.at[step, hop], r2.at[step, hop], near(hop))
+            )
+    for copy in waits:
+        copy.wait()
+
+
+def move_rows(x, inner, scatter):
+    tp = lax.axis_size("tp")
+    shape = x.shape if scatter else (tp, inner) + x.shape
+    sems = pltpu.SemaphoreType.DMA
+    vmem = pl.BlockSpec(memory_space=pltpu.VMEM)
+    return pl.pallas_call(
+        functools.partial(rows_kernel, inner, tp, scatter),
+        in_specs=[vmem],
+        out_specs=vmem,
+        out_shape=jax.ShapeDtypeStruct(shape, x.dtype),
+        scratch_shapes=[
+            sems((inner,)),
+            sems((inner,)),
+            sems((inner, tp)),
+            sems((inner, tp)),
+            sems(()),
+        ],
+        compiler_params=pltpu.CompilerParams(
+            collective_id=1 if scatter else 2, has_side_effects=True
+        ),
+        cost_estimate=pl.CostEstimate(
+            flops=20_000_000_000, bytes_accessed=10_000_000, transcendentals=0
+        ),
+        name="scatter_rows" if scatter else "gather_rows",
+    )(x)
+
+
 def rms_scale(rows, gain):
     x = rows.astype(jnp.float32)
     factor = lax.rsqrt(jnp.mean(x * x, axis=-1, keepdims=True) + NORM_EPS)
@@ -305,8 +388,6 @@
     sp, tp = lax.axis_size("sp"), lax.axis_size("tp")
     fits = sp % INNER == 0 and w_gate.shape[1] % (INNER * LANES) == 0
     inner = INNER if fits else 1
-    outer = sp // inner
-    near = [[i * outer + j for i in range(inner)] for j in range(outer)]
     hidden = w_gate.shape[1] // inner
 
     q, y, ps = recurrence(r, k, v, dw, lw)
@@ -314,6 +395,7 @@
 
     w_gate, w_up, w_down, q = lax.optimization_barrier((w_gate, w_up, w_down, q))
     g_all, u_all, d_all = spread_weights(inner, w_gate, w_up, w_down)
+    y, g_all, u_all, d_all = lax.optimization_barrier((y, g_all, u_all, d_all))
     g_all = g_all.reshape(-1, hidden)
     u_all = u_all.reshape(-1, hidden)
     d_all = jnp.moveaxis(d_all, 0, 1).reshape(hidden, -1)
@@ -328,17 +410,17 @@
     mix = jnp.sum(mix.astype(jnp.float32), axis=0).astype(jnp.bfloat16).astype(jnp.float32)
     mine = lax.dynamic_slice_in_dim(residual, start, own_rows, 0)
     after = (mine.astype(jnp.float32) + mix).astype(jnp.bfloat16)
-    normed = lax.all_gather(rms_scale(after, gain), "tp", axis=0, tiled=True)
-    normed = lax.all_gather(normed, "sp", axis_index_groups=near, axis=0, tiled=True)
+    normed = move_rows(rms_scale(after, gain), inner, False)
+    normed = normed.reshape(tp * inner * own_rows, -1)
     g = jnp.dot(normed, g_all, preferred_element_type=jnp.float32)
     u = jnp.dot(normed, u_all, preferred_element_type=jnp.float32)
     h = (jax.nn.silu(g) * u).astype(jnp.bfloat16)
     down = jnp.dot(h, d_all, preferred_element_type=jnp.float32).astype(jnp.bfloat16)
-    down = down.reshape(inner, tp, own_rows, -1)
-    down = lax.all_to_all(down, "sp", 0, 0, axis_index_groups=near)
-    down = jnp.sum(down.astype(jnp.float32), axis=0).astype(jnp.bfloat16)
-    down = lax.all_to_all(down, "tp", 0, 0)
+    down = lax.all_to_all(down.reshape(tp, inner, own_rows, -1), "tp", 0, 0)
     down = jnp.sum(down.astype(jnp.float32), axis=0)
+    if inner > 1:
+        down = move_rows(down.astype(jnp.bfloat16), inner, True).astype(jnp.float32)
+    down = jnp.sum(down, axis=0)
     return (after.astype(jnp.float32) + down).astype(jnp.bfloat16)
 
 

time: 354 us -> 284 us (0.80); the launches traced: 347 us -> 283 us
  Pallas kernels: 137 us -> 224 us
  blocking collectives: 93.7 us -> 14.3 us
  waiting for transfers between devices: 74.1 us -> 0.02 us
    pallas_call x0 -> x2, Pallas kernels: none -> 84.4 us  [move_rows(): pl.pallas_call(functools.partial(rows_kernel, inner, tp, scatter), in_spe...]
    all_to_all x2 -> x1, blocking collectives: 84.2 us -> 7.31 us  [per_device(): down = lax.all_to_all(down.reshape(tp, inner, own_rows, -1), 'tp', 0, 0)]
    all_gather x1, waiting for transfers between devices: 74 us -> 0.01 us  [per_device(): ps_all = lax.all_gather(ps, 'sp')]
  transfers between devices with their start and end apart: 2 -> 1, of which waited for: 1 -> 0; matrix products, arithmetic and copies ran while one was open for 1% -> 1% of each run, Pallas kernels for 32% -> 40%
where the time goes in v3:
time: 284 us; the launch traced here: 283 us
  Pallas kernels  224 us (79%)
  matrix products  16.5 us (6%)
  blocking collectives  14.3 us (5%)
  between operations  13.5 us (5%)
  local copies, waits for them, and re-layouts  8.36 us (3%)
  other arithmetic  6.27 us (2%)
    pallas_call x1, Pallas kernels, spread_weights(): pl.pallas_call(functools.partial(weights_kernel, inner, outer), in_specs=...  113 us
    pallas_call x2, Pallas kernels, move_rows(): pl.pallas_call(functools.partial(rows_kernel, inner, tp, scatter), in_spe...  84.4 us
    pallas_call x1, Pallas kernels, recurrence(): pl.pallas_call(local_kernel, grid=(pairs,), in_specs=[cols] * 5, out_spec...  19.5 us
    dot_general x1, matrix products, per_device(): jnp.dot(h, d_all, preferred_element_type=jnp.float32).astype(jnp.bfloat16)  9.81 us
    pallas_call x1, Pallas kernels, join(): pl.pallas_call(join_kernel, in_specs=[pl.BlockSpec(memory_space=pltpu.SME...  7.75 us
    all_to_all x1, blocking collectives, per_device(): down = lax.all_to_all(down.reshape(tp, inner, own_rows, -1), 'tp', 0, 0)  7.31 us
    all_to_all x1, blocking collectives, per_device(): mix = lax.all_to_all(part.reshape(tp, own_rows, -1), 'tp', 0, 0)  6.99 us
    dot_general x1, matrix products, per_device(): g = jnp.dot(normed, g_all, preferred_element_type=jnp.float32)  6.73 us
  transfers between devices with their start and end apart: 1, of which 0 were waited for; matrix products, arithmetic and copies ran while one was open for 1% of the time, Pallas kernels for 40%

profile of v3, /device:TPU:15, one launch (start us, length us, event | category | flops | bytes accessed | tf_op | source)
XLA Modules:
  0.0 283.4 jit_solution(8057813852486968059)
XLA Ops:
  6.5 0.0 all-gather.3.cloned.1.call-start
  6.5 19.5 %local_part.1 = (f32[192,512]{1,0:T(8,128)}, f32[192,512]{1,0:T(8,128)}, f32[4,2,64,128]{3,2,1,0:T(8,128)}) custom-call(bf16[192,512]{1,0:T(8,128)(2,1)} %r_ref.3, bf16[192,512]{1,0:T(8,128)(2,1)} %k_ref.3, bf16[192,512]{1,0:T(8,128)(2,1)} %v_ref.3, f32[192,512]{1,0:T(8,128)} %dw_ref.1, f32[192,512]{1,0:T(8,128)} %lw_ref.1), custom_call_target="tpu_custom_call" | custom-call | flops 20000000000 | bytes 4000000 | tf_op jit(solution)/shard_map/local_part/pallas_call | solution.py:176
  26.0 0.0 all-gather.3.cloned.1.call-update
  26.1 0.0 copy-done.8
  26.1 0.6 reshape.37.tw_ref
  26.7 1.1 copy-done.1
  27.8 1.1 copy-done.2
  28.9 112.8 %spread_weights.1 = (bf16[16,128,640]{2,1,0:T(8,128)(2,1)S(1)}, bf16[16,128,640]{2,1,0:T(8,128)(2,1)S(1)}, bf16[16,640,128]{2,1,0:T(8,128)(2,1)S(1)}) custom-call(bf16[128,2560]{1,0:T(8,128)(2,1)S(1)} %copy-done, bf16[128,2560]{1,0:T(8,128)(2,1)S(1)} %copy-done.1, bf16[2560,128]{1,0:T(8,128)(2,1)S(1)} %copy-done.2), custom_call_target="tpu_custom_call" | custom-call | flops 49999998976 | bytes 100000000 | tf_op jit(solution)/shard_map/spread_weights/pallas_call | solution.py:275
  141.7 1.5 copy-done.3
  143.2 1.5 copy-done.5
  144.7 2.6 copy.16
  147.3 7.7 %join_part.1 = bf16[192,2048]{1,0:T(8,128)(2,1)} custom-call(s32[1]{0:T(128)} %bitcast.i_ref, f32[16,4,2,64,128]{4,3,2,1,0:T(8,128)} %bitcast.21, f32[192,512]{1,0:T(8,128)} %get-tuple-element.21.q_ref, f32[192,512]{1,0:T(8,128)} %get-tuple-element.29.y_ref, bf16[192,512]{1,0:T(8,128)(2,1)} %r_ref.3, bf16[192,512]{1,0:T(8,128)(2,1)} %k_ref.3, ...), custom_call_target="tpu_custom_call" | custom-call | flops 10000000000 | bytes 8000000 | tf_op jit(solution)/shard_map/join_part/pallas_call | solution.py:195
  155.0 7.0 %all_to_all.10 = bf16[2,96,2048]{2,1,0:T(8,128)(2,1)S(1)} all-to-all(bf16[2,96,2048]{2,1,0:T(8,128)(2,1)} %bitcast.20), channel_id=1, replica_groups=mesh['sp'=16,'tp'=2] {'tp'}, dimensions={0} | all-to-all | bytes 1572864 | tf_op jit(solution)/shard_map/all_to_all | solution.py:409
  162.0 0.2 reduce_sum.42
  162.2 0.2 fusion
  162.5 0.9 fusion.2.x_ref
  163.4 44.1 %gather_rows.1 = bf16[2,4,96,2048]{3,2,1,0:T(8,128)(2,1)} custom-call(bf16[96,2048]{1,0:T(8,128)(2,1)} %fusion.2.x_ref), custom_call_target="tpu_custom_call" | custom-call | flops 20000000000 | bytes 10000000 | tf_op jit(solution)/shard_map/gather_rows/pallas_call | solution.py:358
  207.5 6.7 %fusion.5 = f32[768,640]{1,0:T(8,128)} fusion(bf16[768,2048]{1,0:T(8,128)(2,1)} %bitcast.23, bf16[2048,640]{1,0:T(8,128)(2,1)} %bitcast.17), kind=kOutput, calls=%fused_computation.13 | convolution fusion | flops 2013265920 | bytes 7733248 | tf_op jit(solution)/shard_map/dot_general | solution.py:415
  214.2 9.8 %convolution_convert_fusion = bf16[768,2048]{1,0:T(8,128)(2,1)} fusion(bf16[640,2048]{0,1:T(8,128)(2,1)} %bitcast.19, f32[768,640]{1,0:T(8,128)} %fusion.5, bf16[768,2048]{1,0:T(8,128)(2,1)} %bitcast.24, bf16[2048,640]{1,0:T(8,128)(2,1)S(1)} %bitcast.16), kind=kOutput, calls=%fused_computation | convolution fusion | flops 4031053824 | bytes 13500416 | tf_op jit(solution)/shard_map/dot_general | solution.py:418
  224.0 7.3 %all_to_all.11 = bf16[2,4,96,2048]{3,2,1,0:T(8,128)(2,1)S(1)} all-to-all(bf16[2,4,96,2048]{3,2,1,0:T(8,128)(2,1)} %bitcast.18), channel_id=1, replica_groups=mesh['sp'=16,'tp'=2] {'tp'}, dimensions={0} | all-to-all | bytes 6291456 | tf_op jit(solution)/shard_map/all_to_all | solution.py:419
  231.4 2.3 reduce_sum.44.x_ref
  233.7 40.3 %scatter_rows.1 = bf16[4,96,2048]{2,1,0:T(8,128)(2,1)} custom-call(bf16[4,96,2048]{2,1,0:T(8,128)(2,1)} %reduce_sum.44.x_ref), custom_call_target="tpu_custom_call" | custom-call | flops 20000000000 | bytes 10000000 | tf_op jit(solution)/shard_map/scatter_rows/pallas_call | solution.py:358
  274.0 1.8 convert_reduce_fusion
  275.8 0.8 fusion.3
  (15 shorter events, 0.0 us)
Async XLA Ops:
  6.5 19.5 %copy-start.8 = (f32[8,64]{1,0:T(8,128)S(1)}, f32[8,64]{1,0:T(8,128)}, u32[]{:S(2)}) copy-start(f32[8,64]{1,0:T(8,128)} %param.20) | copy-start | bytes 6148
  6.5 20.1 %copy-start = (bf16[128,2560]{1,0:T(8,128)(2,1)S(1)}, bf16[128,2560]{1,0:T(8,128)(2,1)}, u32[]{:S(2)}) copy-start(bf16[128,2560]{1,0:T(8,128)(2,1)} %g_ref.1) | copy-start | bytes 1966084
  6.5 140.7 %all-gather.3.cloned.1.call-start = ((), (), s32[]{:S(2)}) async-start(), calls=%async_computation.2 | async-start | bytes 4456448 | tf_op jit(solution)/shard_map/all_gather | solution.py:394
  26.7 1.1 copy-start.1
  27.8 1.1 copy-start.2
  141.7 1.5 copy-start.3
  143.2 1.5 copy-start.5
  155.0 7.2 %copy-start.6 = (bf16[192,2048]{1,0:T(8,128)(2,1)S(1)}, bf16[192,2048]{1,0:T(8,128)(2,1)}, u32[]{:S(2)}) copy-start(bf16[192,2048]{1,0:T(8,128)(2,1)} %param.23) | copy-start | bytes 2359300
  155.0 7.4 %copy-start.7 = (f32[2048]{0:T(1024)S(1)}, f32[2048]{0:T(1024)}, u32[]{:S(2)}) copy-start(f32[2048]{0:T(1024)} %param.24) | copy-start | bytes 24580
  207.5 6.7 %copy-start.4 = (bf16[16,128,640]{2,1,0:T(8,128)(2,1)S(1)}, bf16[16,128,640]{2,1,0:T(8,128)(2,1)}, u32[]{:S(2)}) copy-start(bf16[16,128,640]{2,1,0:T(8,128)(2,1)} %copy-done.3) | copy-start | bytes 7864324
Sparse Core Ops, SparseCore 0:
  26.2 120.8 all-gather.2
